TPU v7x, 32 devices: a whole 2x2x4 slice. The times are simulated.
32 devices in a mesh: sp: 8 (over z, core), tp: 4 (over y, x).
Axes of the slice: x: 2, y: 2, z: 4, core: 2. Of those that a mesh axis runs over, the one named last changes fastest.
Arguments:
- queries: bfloat16 [2048, 1024], P('sp', 'tp'), may hold values from -250 to 250
- keys_values: bfloat16 [2, 2048, 256], P(None, 'sp'), may hold values from -8 to 8
- sink_logits: float32 [16], P('tp'), may hold values from 1 to 5
- proj_weight: bfloat16 [1024, 2048], P('tp'), may hold values from -0.75 to 0.75
- residual: bfloat16 [2048, 2048], P('sp', 'tp'), may hold values from -6 to 6
- norm_gain: float32 [2048], replicated, may hold values from 0.1 to 1.9
- routes: int32 [2048, 2], P('sp'), may hold values from 0 to 7, all different within a row; in each aligned block of 256 rows (0 to 255, 256 to 511, ...) at most 128 rows name the same one
- route_weights: float32 [2048, 2], P('sp'), may hold values from 0.2 to 1
- gate_weight: bfloat16 [8, 2048, 2048], P('sp', None, 'tp'), may hold values from -0.125 to 0.125
- up_weight: bfloat16 [8, 2048, 2048], P('sp', None, 'tp'), may hold values from -0.125 to 0.125
- down_weight: bfloat16 [8, 2048, 2048], P('sp', None, 'tp'), may hold values from -0.125 to 0.125
- shared_gate: bfloat16 [2048, 2048], P(None, 'tp'), may hold values from -0.125 to 0.125
- shared_up: bfloat16 [2048, 2048], P(None, 'tp'), may hold values from -0.125 to 0.125
- shared_down: bfloat16 [2048, 2048], P(None, 'tp'), may hold values from -0.125 to 0.125
Outputs:
- output: bfloat16 [2048, 2048], P('sp', 'tp')
Inputs may be any that keep to these rules, and one draw needn't show every extreme that they name: `routes`: the 2 experts of a position differ. In each aligned block of 256 positions no expert is named by more than 128 positions, and in some block one expert is named by exactly 128.
All inputs are finite; a program needn't handle non-finite values.
Results may differ from a plain program's by a relative error of at most 0.0067.
Values may be sent and summed in bfloat16 or wider, within the bound.
A program may use at most 64 MiB of HBM per device.

v0:
```python
import jax
import jax.numpy as jnp
from jax import lax
from jax.sharding import PartitionSpec as P

D = 2048
HEADS = 16
KV_HEADS = 4
HEAD_WIDTH = 64
WINDOW = 128
TOP_K = 2
EXP_DEV = 1
TOK_DEV = 256


norm_eps = 1e-06


def passed_along(value, axis, steps):
    count = lax.axis_size(axis)
    initial, last = (max(0, -steps), min(count, count - steps))
    return lax.ppermute(value, axis, [(source, source + steps) for source in range(initial, last)])


def per_device(
    queries,
    keys_values,
    sink_logits,
    proj_weight,
    residual,
    norm_gain,
    routes,
    route_weights,
    gate_weight,
    up_weight,
    down_weight,
    shared_gate,
    shared_up,
    shared_down,
):
    tp_index = lax.axis_index("tp")
    sp_index = lax.axis_index("sp")
    sp_count = lax.axis_size("sp")
    tp_count = lax.axis_size("tp")
    heads_here = sink_logits.shape[0]
    col_width = residual.shape[1]
    blocks = TOK_DEV // WINDOW
    kv_group = HEADS // KV_HEADS
    earlier_keys = passed_along(keys_values[:, TOK_DEV - WINDOW :, :], "sp", 1)
    extended = jnp.concatenate([earlier_keys, keys_values], axis=1)
    extended = extended.reshape(2, TOK_DEV + WINDOW, KV_HEADS, HEAD_WIDTH)
    head_ids = tp_index * heads_here + jnp.arange(heads_here, dtype=jnp.int32)
    chosen = jnp.take(extended, head_ids // kv_group, axis=2)
    earlier = chosen[:, :TOK_DEV].reshape(2, blocks, WINDOW, heads_here, HEAD_WIDTH)
    later = chosen[:, WINDOW:].reshape(2, blocks, WINDOW, heads_here, HEAD_WIDTH)
    banded = jnp.concatenate([earlier, later], axis=2)
    query_blocks = queries.reshape(blocks, WINDOW, heads_here, HEAD_WIDTH)
    score_matrix = jnp.einsum(
        "bqhd,bkhd->bhqk", query_blocks, banded[0], preferred_element_type=jnp.float32
    ) * HEAD_WIDTH ** (-0.5)
    query_pos = jnp.arange(WINDOW, dtype=jnp.int32)[:, None]
    key_pos = jnp.arange(2 * WINDOW, dtype=jnp.int32)[None, :]
    distance = WINDOW + query_pos - key_pos
    absolute = (
        sp_index * TOK_DEV
        + jnp.arange(blocks, dtype=jnp.int32)[:, None, None] * WINDOW
        - WINDOW
        + key_pos[None]
    )
    allowed = (distance >= 0)[None] & (distance < WINDOW)[None] & (absolute >= 0)
    masked = jnp.where(allowed[:, None], score_matrix, -jnp.inf)
    sink_value = sink_logits[None, :, None, None]
    highest = jnp.maximum(jnp.max(masked, axis=-1, keepdims=True), sink_value)
    weights_exp = jnp.exp(masked - highest)
    denominator = jnp.sum(weights_exp, axis=-1, keepdims=True) + jnp.exp(sink_value - highest)
    softmax_weights = (weights_exp / denominator).astype(jnp.bfloat16)
    attended_values = jnp.einsum(
        "bhqk,bkhd->bqhd", softmax_weights, banded[1], preferred_element_type=jnp.float32
    )
    attended_values = attended_values.astype(jnp.bfloat16).reshape(TOK_DEV, heads_here * HEAD_WIDTH)
    attended_all = lax.all_gather(attended_values, "tp", axis=1, tiled=True)
    weight_rows = proj_weight.shape[0]
    column_share = lax.all_to_all(
        proj_weight.reshape(weight_rows, tp_count, col_width),
        "tp",
        split_axis=1,
        concat_axis=0,
        tiled=True,
    )
    column_share = column_share.reshape(HEADS * HEAD_WIDTH, col_width)
    feature_sum = jnp.dot(attended_all, column_share, preferred_element_type=jnp.float32)
    stream_cols = (feature_sum + residual.astype(jnp.float32)).astype(jnp.bfloat16)
    stream_rows = lax.all_gather(stream_cols, "tp", axis=1, tiled=True)
    gate_eff = (norm_gain[None, :, None] * gate_weight.astype(jnp.float32)).astype(jnp.bfloat16)
    up_eff = (norm_gain[None, :, None] * up_weight.astype(jnp.float32)).astype(jnp.bfloat16)
    shared_gate_eff = (norm_gain[:, None] * shared_gate.astype(jnp.float32)).astype(jnp.bfloat16)
    shared_up_eff = (norm_gain[:, None] * shared_up.astype(jnp.float32)).astype(jnp.bfloat16)
    experts_total = EXP_DEV * sp_count
    capacity = 2 * TOK_DEV * TOP_K // experts_total
    rows_per_expert = sp_count * capacity
    flat_routes = routes.reshape(-1)
    onehot = (flat_routes[:, None] == jnp.arange(experts_total, dtype=jnp.int32)[None, :]).astype(
        jnp.int32
    )
    before = jnp.cumsum(onehot, axis=0) - onehot
    slot_rank = jnp.sum(before * onehot, axis=1)
    slot_index = (
        flat_routes % EXP_DEV * rows_per_expert + flat_routes // EXP_DEV * capacity + slot_rank
    )
    token_of = jnp.arange(TOK_DEV * TOP_K, dtype=jnp.int32) // TOP_K
    slot_owner = (
        jnp.full((EXP_DEV * rows_per_expert,), TOK_DEV, jnp.int32).at[slot_index].set(token_of)
    )
    picked_rows = jnp.take(stream_rows, slot_owner, axis=0, mode="fill", fill_value=0)
    arrived = lax.all_to_all(
        picked_rows.reshape(EXP_DEV, sp_count, capacity, stream_rows.shape[1]),
        "sp",
        split_axis=1,
        concat_axis=1,
        tiled=True,
    )
    arrived = arrived.reshape(EXP_DEV, rows_per_expert, D)
    routed_squares = jnp.sum(jnp.square(arrived.astype(jnp.float32)), axis=-1)
    gate_sum = jnp.einsum("erd,edf->erf", arrived, gate_eff, preferred_element_type=jnp.float32)
    up_sum = jnp.einsum("erd,edf->erf", arrived, up_eff, preferred_element_type=jnp.float32)
    own_squares = jnp.sum(jnp.square(stream_rows.astype(jnp.float32)), axis=-1)
    shared_gate_sum = jnp.dot(stream_rows, shared_gate_eff, preferred_element_type=jnp.float32)
    shared_up_sum = jnp.dot(stream_rows, shared_up_eff, preferred_element_type=jnp.float32)
    routed_scale = lax.rsqrt(routed_squares / D + norm_eps)[..., None]
    own_scale = lax.rsqrt(own_squares / D + norm_eps)[:, None]
    hidden = (jax.nn.silu(routed_scale * gate_sum) * (routed_scale * up_sum)).astype(jnp.bfloat16)
    shared_hidden = (jax.nn.silu(own_scale * shared_gate_sum) * (own_scale * shared_up_sum)).astype(
        jnp.bfloat16
    )
    routed_piece = lax.all_gather(hidden, "tp", axis=2, tiled=True)
    own_piece = lax.all_gather(shared_hidden[None], "tp", axis=2, tiled=True)
    expert_out = jnp.einsum(
        "erf,efd->erd", routed_piece, down_weight, preferred_element_type=jnp.float32
    )
    shared_out = jnp.dot(own_piece[0], shared_down, preferred_element_type=jnp.float32)
    outgoing = expert_out.astype(jnp.bfloat16).reshape(EXP_DEV, sp_count, capacity, col_width)
    returned = lax.all_to_all(outgoing, "sp", split_axis=1, concat_axis=1, tiled=True).reshape(
        EXP_DEV * rows_per_expert, col_width
    )
    picked = jnp.take(returned, slot_index, axis=0).reshape(TOK_DEV, TOP_K, col_width)
    routed_sum = jnp.einsum("nk,nkd->nd", route_weights, picked.astype(jnp.float32))
    return (stream_cols.astype(jnp.float32) + shared_out + routed_sum).astype(jnp.bfloat16)


def solution(mesh):
    placed = (
        P("sp", "tp"),
        P(None, "sp", None),
        P("tp"),
        P("tp", None),
        P("sp", "tp"),
        P(),
        P("sp", None),
        P("sp", None),
        P("sp", None, "tp"),
        P("sp", None, "tp"),
        P("sp", None, "tp"),
        P(None, "tp"),
        P(None, "tp"),
        P(None, "tp"),
    )
    return jax.shard_map(
        per_device, mesh=mesh, in_specs=placed, out_specs=P("sp", "tp"), check_vma=False
    )
```

profile of v0, /device:TPU:0, one launch (start us, length us, event | category | flops | bytes accessed | tf_op | source)
XLA Modules:
  0.0 293.3 jit_solution(9455327325811044780)
XLA Ops:
  6.5 1.2 copy.63
  7.8 3.2 %collective-permute-start = (bf16[2,128,256]{1,2,0:T(8,128)(2,1)S(1)}, bf16[2,128,256]{1,2,0:T(8,128)(2,1)}, u32[]{:S(2)}, u32[]{:S(2)}) collective-permute-start(bf16[2,128,256]{1,2,0:T(8,128)(2,1)S(1)} %slice.34), channel_id=1, source_target_pairs={{0,4},{4,8},{8,12},{12,16},{16,20},{20,24},{24,28},{1,5},{5,9},{9,... | collective-permute-start | bytes 393224 | tf_op jit(solution)/shard_map/ppermute | solution.py:22
  11.0 2.3 copy.73
  13.3 4.5 %all-to-all-start = ((bf16[256,4,512]{0,2,1:T(8,128)(2,1)}), bf16[256,4,512]{0,2,1:T(8,128)(2,1)S(1)}, u32[]{:S(2)}, u32[]{:S(2)}) async-start(bf16[256,4,512]{0,2,1:T(8,128)(2,1)} %bitcast.91), calls=%async_computation | async-start | bytes 2097152 | tf_op jit(solution)/shard_map/all_to_all | solution.py:83
  18.7 0.9 reshape.384
  19.6 1.0 pad_maximum_fusion
  20.7 1.4 gather_fusion
  22.0 1.1 select_bitcast_fusion
  24.0 1.0 reshape.382
  25.8 1.0 reshape.383
  27.6 1.5 fusion.48
  30.0 12.7 %all_gather.12 = bf16[256,1024]{0,1:T(8,128)(2,1)} all-gather(bf16[256,256]{0,1:T(8,128)(2,1)S(1)} %bitcast.95), channel_id=1, replica_groups=mesh['sp'=8,'tp'=4] {'tp'}, dimensions={1}, use_global_device_ids=true | all-gather | bytes 655360 | tf_op jit(solution)/shard_map/all_gather | solution.py:81
  42.7 1.3 copy.74
  44.0 2.6 fusion.25
  47.1 1.1 reduce-window.6
  48.9 2.4 scatter_custom_fusion
  51.4 20.4 %all-gather.6.cloned.1.call-done = bf16[256,2048]{1,0:T(8,128)(2,1)} async-done(((bf16[256,512]{1,0:T(8,128)(2,1)}), bf16[256,2048]{1,0:T(8,128)(2,1)}) %all-gather.6.cloned.1.call-update) | async-done | bytes 1048592 | tf_op jit(solution)/shard_map/all_gather | solution.py:93
  71.8 10.2 %gather_fusion.1 = bf16[1024,2048]{1,0:T(8,128)(2,1)} fusion(bf16[256,2048]{1,0:T(8,128)(2,1)} %all-gather.6.cloned.1.call-done, s32[1024]{0:T(1024)S(1)} %fusion.39), kind=kCustom, calls=%fused_computation.1 | custom fusion | bytes 8392704 | tf_op jit(solution)/shard_map/jit(_take)/gather | solution.py:114
  82.0 2.5 broadcast_select_fusion
  84.5 98.4 %all_to_all.25 = bf16[1,8,128,2048]{3,2,0,1:T(8,128)(2,1)S(1)} all-to-all(bf16[1,8,128,2048]{3,2,0,1:T(8,128)(2,1)S(1)} %broadcast_select_fusion), channel_id=1, replica_groups=mesh['sp'=8,'tp'=4] {'sp'}, dimensions={1} | all-to-all | bytes 8388608 | tf_op jit(solution)/shard_map/all_to_all | solution.py:115
  182.9 0.9 multiply_reduce_fusion
  184.5 2.4 fusion.3
  186.9 3.7 %multiply_convert_fusion.6 = bf16[1024,512]{1,0:T(8,128)(2,1)} fusion(f32[1024,512]{1,0:T(8,128)S(1)} %fusion.3, bf16[1024,2048]{1,0:T(8,128)(2,1)S(1)} %bitcast.89, bf16[1,2048,512]{2,1,0:T(8,128)(2,1)S(1)} %copy-done.11, f32[2048]{0:T(1024)S(1)} %copy-done.14, f32[1024]{0:T(1024)S(1)} %rsqrt_bitcast_fusion), kind=kOutput, calls=%fused_computation.18 | convolution fusion | flops 2154823680 | bytes 9449472 | tf_op jit(solution)/shard_map/erd,edf->erf/dot_general | solution.py:125
  191.0 50.3 %all-gather.10.cloned.1.call-done = bf16[1024,2048]{1,0:T(8,128)(2,1)} async-done(((bf16[1024,512]{1,0:T(8,128)(2,1)}), bf16[1024,2048]{1,0:T(8,128)(2,1)}) %all-gather.10.cloned.1.call-update) | async-done | bytes 4194320 | tf_op jit(solution)/shard_map/all_gather | solution.py:135
  241.3 5.5 %fusion.16 = bf16[1024,512]{1,0:T(8,128)(2,1)} fusion(bf16[1024,2048]{1,0:T(8,128)(2,1)} %all-gather.10.cloned.1.call-done, bf16[1,2048,512]{2,1,0:T(8,128)(2,1)S(1)} %copy-done), kind=kOutput, calls=%fused_computation.24 | convolution fusion | flops 2148007936 | bytes 7340032 | tf_op jit(solution)/shard_map/erf,efd->erd/dot_general | solution.py:137
  246.8 4.6 %all-to-all-start.2 = ((bf16[1,8,128,512]{3,2,0,1:T(8,128)(2,1)}), bf16[1,8,128,512]{3,2,0,1:T(8,128)(2,1)}, u32[]{:S(2)}, u32[]{:S(2)}) async-start(bf16[1,8,128,512]{3,2,0,1:T(8,128)(2,1)} %bitcast.93), calls=%async_computation.2 | async-start | bytes 2097152 | tf_op jit(solution)/shard_map/all_to_all | solution.py:142
  251.4 2.6 fusion.23
  254.0 1.6 fusion.27
  256.3 21.8 %all-to-all-done.2 = bf16[1,8,128,512]{3,2,0,1:T(8,128)(2,1)} async-done(((bf16[1,8,128,512]{3,2,0,1:T(8,128)(2,1)}), bf16[1,8,128,512]{3,2,0,1:T(8,128)(2,1)}, u32[]{:S(2)}, u32[]{:S(2)}) %all-to-all-start.2) | async-done | bytes 1048608 | tf_op jit(solution)/shard_map/all_to_all | solution.py:142
  278.0 3.3 %gather_fusion.2 = bf16[512,512]{1,0:T(8,128)(2,1)S(1)} fusion(bf16[1024,512]{1,0:T(8,128)(2,1)} %bitcast.25, s32[1024]{0:T(1024)S(1)} %pad_clamp_fusion), kind=kCustom, calls=%fused_computation.2 | custom fusion | bytes 1050624 | tf_op jit(solution)/shard_map/jit(_take)/gather | solution.py:145
  281.6 1.8 fusion.30
  283.4 3.4 %fusion.26 = bf16[256,512]{1,0:T(8,128)(2,1)} fusion(bf16[256,2048]{1,0:T(8,128)(2,1)} %all-gather.8.cloned.1.call-done, bf16[2048,512]{1,0:T(8,128)(2,1)} %param.27, f32[256,1,512]{2,1,0:T(1,128)} %fusion.30, bf16[256,512]{1,0:T(8,128)(2,1)S(1)} %copy-done.3), kind=kOutput, calls=%fused_computation.35 | convolution fusion | flops 537395200 | bytes 4194304 | tf_op jit(solution)/shard_map/dot_general | solution.py:140
  (82 shorter events, 7.2 us)
Async XLA Ops:
  6.5 234.7 %copy-start = (bf16[1,2048,512]{2,1,0:T(8,128)(2,1)S(1)}, bf16[1,2048,512]{2,1,0:T(8,128)(2,1)}, u32[]{:S(2)}) copy-start(bf16[1,2048,512]{2,1,0:T(8,128)(2,1)} %param.24) | copy-start | bytes 6291460
  7.8 5.5 %copy-start.2 = (bf16[2,256,256]{1,2,0:T(8,128)(2,1)}, bf16[2,256,256]{1,2,0:T(8,128)(2,1)S(1)}, u32[]{:S(2)}) copy-start(bf16[2,256,256]{1,2,0:T(8,128)(2,1)S(1)} %copy.63) | copy-start | bytes 786436
  7.8 10.9 %copy-start.4 = (bf16[256,256]{1,0:T(8,128)(2,1)S(1)}, bf16[256,256]{1,0:T(8,128)(2,1)}, u32[]{:S(2)}) copy-start(bf16[256,256]{1,0:T(8,128)(2,1)} %param.14) | copy-start | bytes 393220
  7.8 11.8 %collective-permute-start = (bf16[2,128,256]{1,2,0:T(8,128)(2,1)S(1)}, bf16[2,128,256]{1,2,0:T(8,128)(2,1)}, u32[]{:S(2)}, u32[]{:S(2)}) collective-permute-start(bf16[2,128,256]{1,2,0:T(8,128)(2,1)S(1)} %slice.34), channel_id=1, source_target_pairs={{0,4},{4,8},{8,12},{12,16},{16,20},{20,24},{24,28},{1,5},{5,9},{9,... | collective-permute-start | bytes 393224 | tf_op jit(solution)/shard_map/ppermute | solution.py:22
  13.3 29.4 %all-to-all-start = ((bf16[256,4,512]{0,2,1:T(8,128)(2,1)}), bf16[256,4,512]{0,2,1:T(8,128)(2,1)S(1)}, u32[]{:S(2)}, u32[]{:S(2)}) async-start(bf16[256,4,512]{0,2,1:T(8,128)(2,1)} %bitcast.91), calls=%async_computation | async-start | bytes 2097152 | tf_op jit(solution)/shard_map/all_to_all | solution.py:83
  17.8 54.0 %all-gather.6.cloned.1.call-start = ((), (), s32[]{:S(2)}) async-start(), calls=%async_computation.3 | async-start | bytes 1310720 | tf_op jit(solution)/shard_map/all_gather | solution.py:93
  22.0 5.6 %copy-start.6 = (pred[2,128,256]{1,2,0:T(8,128)(4,1)S(1)}, pred[2,128,256]{1,2,0:T(8,128)(4,1)}, u32[]{:S(2)}) copy-start(pred[2,128,256]{1,2,0:T(8,128)(4,1)} %broadcast_and_fusion) | copy-start | bytes 196612
  24.0 5.1 %copy-start.9 = (f32[4]{0:T(128)S(1)}, f32[4]{0:T(128)}, u32[]{:S(2)}) copy-start(f32[4]{0:T(128)} %param.16) | copy-start | bytes 52
  27.6 1.8 copy-start.5
  29.8 14.3 %copy-start.13 = (bf16[256,512]{1,0:T(8,128)(2,1)S(1)}, bf16[256,512]{1,0:T(8,128)(2,1)}, u32[]{:S(2)}) copy-start(bf16[256,512]{1,0:T(8,128)(2,1)} %param.18) | copy-start | bytes 786436
  42.7 4.0 %copy-start.7 = (s32[256,2]{0,1:T(2,128)S(1)}, s32[256,2]{0,1:T(2,128)}, u32[]{:S(2)}) copy-start(s32[256,2]{0,1:T(2,128)} %param.20) | copy-start | bytes 6148
  46.6 194.7 %all-gather.10.cloned.1.call-start = ((), (), s32[]{:S(2)}) async-start(), calls=%async_computation.5 | async-start | bytes 5242880 | tf_op jit(solution)/shard_map/all_gather | solution.py:135
  182.9 1.6 copy-start.10
  182.9 1.6 copy-start.14
  184.5 2.4 copy-start.11
  186.9 3.8 %copy-start.1 = (bf16[256,2048]{1,0:T(8,128)(2,1)S(1)}, bf16[256,2048]{1,0:T(8,128)(2,1)}, u32[]{:S(2)}) copy-start(bf16[256,2048]{1,0:T(8,128)(2,1)} %all-gather.6.cloned.1.call-done) | copy-start | bytes 3145732
  246.8 31.3 %all-to-all-start.2 = ((bf16[1,8,128,512]{3,2,0,1:T(8,128)(2,1)}), bf16[1,8,128,512]{3,2,0,1:T(8,128)(2,1)}, u32[]{:S(2)}, u32[]{:S(2)}) async-start(bf16[1,8,128,512]{3,2,0,1:T(8,128)(2,1)} %bitcast.93), calls=%async_computation.2 | async-start | bytes 2097152 | tf_op jit(solution)/shard_map/all_to_all | solution.py:142
  251.4 32.0 %all-gather.8.cloned.1.call-start = ((), (), s32[]{:S(2)}) async-start(), calls=%async_computation.4 | async-start | bytes 1310720 | tf_op jit(solution)/shard_map/all_gather | solution.py:136
  251.4 2.6 copy-start.12
  254.0 2.1 copy-start.8
  281.6 1.8 copy-start.3
Sparse Core Ops, SparseCore 0:
  46.7 25.0 all-gather.5
  190.8 50.3 all-gather.9
  255.8 26.7 all-gather.7
where the time goes:
time: 294 us; the launch traced here: 293 us
  blocking collectives  111 us (38%)
  waiting for transfers between devices  92.4 us (31%)
  local copies, waits for them, and re-layouts  30.1 us (10%)
  matrix products  25.3 us (9%)
  between operations  13.5 us (5%)
  starting transfers between devices  12.4 us (4%)
  other arithmetic  8.46 us (3%)
    all_to_all x1, blocking collectives, per_device(): lax.all_to_all(picked_rows.reshape(EXP_DEV, sp_count, capacity, stream_ro...  98.4 us
    all_gather x1, waiting for transfers between devices, per_device(): routed_piece = lax.all_gather(hidden, 'tp', axis=2, tiled=True)  50.3 us
    all_to_all x1, waiting for transfers between devices, per_device(): lax.all_to_all(outgoing, 'sp', split_axis=1, concat_axis=1, tiled=True)  21.8 us
    all_gather x1, waiting for transfers between devices, per_device(): stream_rows = lax.all_gather(stream_cols, 'tp', axis=1, tiled=True)  20.4 us
    all_gather x1, blocking collectives, per_device(): attended_all = lax.all_gather(attended_values, 'tp', axis=1, tiled=True)  12.7 us
    gather x1, local copies, waits for them, and re-layouts, per_device(): jnp.take(stream_rows, slot_owner, axis=0, mode='fill', fill_value=0)  10.2 us
  transfers between devices with their start and end apart: 6, of which 3 were waited for; matrix products, arithmetic and copies ran while one was open for 10% of the time, Pallas kernels for 0%

commit v1 on v0

v1 whole, which is shorter than its diff:
```python
import functools

import jax
import jax.numpy as jnp
from jax import lax
from jax.experimental import pallas as pl
from jax.experimental.pallas import tpu as pltpu
from jax.sharding import PartitionSpec as P

D = 2048
HEADS = 16
KV_HEADS = 4
HEAD_WIDTH = 64
WINDOW = 128
TOP_K = 2
EXP_DEV = 1
TOK_DEV = 256


norm_eps = 1e-06


def passed_along(value, axis, steps):
    count = lax.axis_size(axis)
    initial, last = (max(0, -steps), min(count, count - steps))
    return lax.ppermute(value, axis, [(source, source + steps) for source in range(initial, last)])


MESH = pl.DeviceIdType.MESH
CORES = 2
LAG = 3


def expert_kernel(
    sp_count,
    tp_count,
    cap,
    stream_ref,
    routes_ref,
    routes_row_ref,
    weights_ref,
    gain_ref,
    gate_ref,
    up_ref,
    down_ref,
    sgate_ref,
    sup_ref,
    sdown_ref,
    out_ref,
    wgu,
    wd,
    sgu,
    sd,
    full,
    picks,
    picked_full,
    arrived,
    hid,
    shid,
    eout,
    returned,
    pos,
    acc,
    load_sem,
    stream_sems,
    z_send,
    z_recv,
    fwd_send,
    fwd_recv,
    hid_send,
    hid_recv,
    sh_sems,
    ret_send,
    ret_recv,
):
    s = lax.axis_index("sp")
    t = lax.axis_index("tp")
    rows, width = stream_ref.shape
    depth = width * tp_count
    chips = sp_count // CORES
    z, core = s // CORES, lax.rem(s, CORES)
    cols = pl.ds(pl.multiple_of(t * width, width), width)
    wide = pl.ds(0, (tp_count - 1) * width)

    def source(i):
        return lax.rem(z + i // CORES, chips) * CORES + lax.rem(core + lax.rem(i, CORES), CORES)

    def target(i):
        return (
            lax.rem(z - i // CORES + chips, chips) * CORES
            + lax.rem(core - lax.rem(i, CORES) + CORES, CORES)
        )

    def tp_copies(ref, send_sem, recv_sem):
        for j in range(1, tp_count):
            pltpu.make_async_remote_copy(
                src_ref=ref,
                dst_ref=ref,
                send_sem=send_sem,
                recv_sem=recv_sem,
                device_id={"tp": lax.rem(t + j, tp_count)},
                device_id_type=MESH,
            ).start()

    def tp_wait(ref, send_sem, recv_sem):
        return pltpu.make_async_remote_copy(
            src_ref=ref,
            dst_ref=ref,
            send_sem=send_sem,
            recv_sem=recv_sem,
            device_id={"tp": lax.rem(t + 1, tp_count)},
            device_id_type=MESH,
        )

    def sp_copy(src, dst, send_sem, recv_sem, device):
        return pltpu.make_async_remote_copy(
            src_ref=src,
            dst_ref=dst,
            send_sem=send_sem,
            recv_sem=recv_sem,
            device_id={"sp": device},
            device_id_type=MESH,
        )

    left, right = pl.ds(0, width), pl.ds(width, width)
    loads = [
        pltpu.make_async_copy(src, dst, load_sem.at[n])
        for n, (src, dst) in enumerate(
            (
                (gate_ref.at[0], wgu.at[:, left]),
                (up_ref.at[0], wgu.at[:, right]),
                (sgate_ref, sgu.at[:, left]),
                (sup_ref, sgu.at[:, right]),
                (down_ref.at[0], wd),
                (sdown_ref, sd),
            )
        )
    ]
    for load in loads:
        load.start()

    barrier = pltpu.get_barrier_semaphore()
    for j in range(1, tp_count):
        pl.semaphore_signal(
            barrier, inc=1, device_id={"tp": lax.rem(t + j, tp_count)}, device_id_type=MESH
        )

    @pl.loop(1, sp_count)
    def _(i):
        pl.semaphore_signal(
            barrier, inc=1, device_id={"sp": lax.rem(s + i, sp_count)}, device_id_type=MESH
        )

    full[:, cols] = stream_ref[...]

    named = lax.broadcasted_iota(jnp.int32, (sp_count, rows), 0)
    member = named == routes_row_ref[0:1, :]
    for k in range(1, routes_row_ref.shape[0]):
        member = member | (named == routes_row_ref[k : k + 1, :])
    earlier = lax.broadcasted_iota(jnp.int32, (rows, rows), 0) < lax.broadcasted_iota(
        jnp.int32, (rows, rows), 1
    )
    rank = jnp.dot(
        jnp.where(member, 1.0, 0.0).astype(jnp.bfloat16),
        jnp.where(earlier, 1.0, 0.0).astype(jnp.bfloat16),
        preferred_element_type=jnp.float32,
    )
    pos[...] = jnp.where(member, rank.astype(jnp.int32), -1)

    def chooser(e):
        hit = lax.broadcasted_iota(jnp.int32, (cap, rows), 0) == pos[pl.ds(e, 1), :]
        return jnp.where(hit, 1.0, 0.0).astype(jnp.bfloat16)

    pl.semaphore_wait(barrier, sp_count + tp_count - 2)

    tp_copies(full.at[:, cols], stream_sems.at[0], stream_sems.at[1])

    @pl.loop(CORES, sp_count)
    def _(i):
        e = target(i)
        picks[e] = jnp.dot(
            chooser(e), stream_ref[...], preferred_element_type=jnp.float32
        ).astype(jnp.bfloat16)
        sp_copy(picks.at[e], arrived.at[s, :, cols], z_send.at[e], z_recv.at[s], e).start()

    def scale_weights(w):
        step = 128

        @pl.loop(0, depth // step)
        def _(r):
            part = pl.ds(pl.multiple_of(r * step, step), step)
            w[part, :] = (gain_ref[part, :] * w[part, :].astype(jnp.float32)).astype(jnp.bfloat16)

    loads[0].wait()
    loads[1].wait()
    scale_weights(wgu)

    stream_wait = tp_wait(full.at[:, wide], stream_sems.at[0], stream_sems.at[1])
    stream_wait.wait_recv()
    sibling = target(1)
    picked_full[...] = jnp.dot(
        chooser(sibling), full[...], preferred_element_type=jnp.float32
    ).astype(jnp.bfloat16)
    sp_copy(picked_full, arrived.at[s], z_send.at[sibling], z_recv.at[s], sibling).start()
    arrived[s] = jnp.dot(chooser(s), full[...], preferred_element_type=jnp.float32).astype(
        jnp.bfloat16
    )

    def gated(x, w):
        wide_x = x.astype(jnp.float32)
        scale = lax.rsqrt(jnp.sum(wide_x * wide_x, axis=-1, keepdims=True) / depth + norm_eps)
        sums = jnp.dot(x, w[...], preferred_element_type=jnp.float32)
        gate = scale * sums[:, :width]
        return (gate / (1.0 + jnp.exp(-gate)) * (scale * sums[:, width:])).astype(jnp.bfloat16)

    def hidden_of(src):
        hid[src, :, cols] = gated(arrived[src], wgu)
        tp_copies(hid.at[src, :, cols], hid_send.at[src], hid_recv.at[src])

    hidden_of(s)
    loads[2].wait()
    loads[3].wait()
    scale_weights(sgu)
    half = rows // 2

    @pl.loop(0, 2)
    def _(h):
        part = pl.ds(pl.multiple_of(h * half, half), half)
        shid[part, cols] = gated(full[part, :], sgu)

    tp_copies(shid.at[:, cols], sh_sems.at[0], sh_sems.at[1])

    @pl.loop(CORES, sp_count)
    def _(i):
        src = source(i)
        mine = arrived.at[src, :, cols]
        sp_copy(mine, mine, z_send.at[src], z_recv.at[src], src).wait_recv()
        tp_copies(mine, fwd_send.at[src], fwd_recv.at[src])

    loads[4].wait()
    loads[5].wait()

    @pl.loop(1, sp_count + LAG)
    def _(i):
        @pl.when(i < sp_count)
        def _():
            src = source(i)

            @pl.when(i < CORES)
            def _():
                mine = arrived.at[src]
                sp_copy(mine, mine, z_send.at[src], z_recv.at[src], src).wait_recv()

            @pl.when(i >= CORES)
            def _():
                tp_wait(
                    arrived.at[src, :, wide], fwd_send.at[src], fwd_recv.at[src]
                ).wait_recv()

            hidden_of(src)

        @pl.when(i >= LAG)
        def _():
            src = source(i - LAG)
            tp_wait(hid.at[src, :, wide], hid_send.at[src], hid_recv.at[src]).wait_recv()
            result = jnp.dot(hid[src], wd[...], preferred_element_type=jnp.float32).astype(
                jnp.bfloat16
            )

            @pl.when(i == LAG)
            def _():
                returned[s] = result

            @pl.when(i > LAG)
            def _():
                eout[src] = result
                sp_copy(
                    eout.at[src], returned.at[s], ret_send.at[src], ret_recv.at[s], src
                ).start()

    tp_wait(shid.at[:, wide], sh_sems.at[0], sh_sems.at[1]).wait_recv()
    acc[...] = stream_ref[...].astype(jnp.float32) + jnp.dot(
        shid[...], sd[...], preferred_element_type=jnp.float32
    )

    @pl.loop(0, sp_count)
    def _(i):
        e = target(i)

        @pl.when(i > 0)
        def _():
            mine = returned.at[e]
            sp_copy(mine, mine, ret_send.at[e], ret_recv.at[e], e).wait_recv()

        picked = lax.dot_general(
            chooser(e), returned[e], (((0,), (0,)), ((), ())), preferred_element_type=jnp.float32
        )
        weight = jnp.sum(
            jnp.where(routes_ref[...] == e, weights_ref[...], 0.0), axis=1, keepdims=True
        )
        acc[...] += weight * picked

    out_ref[...] = acc[...].astype(out_ref.dtype)

    stream_wait.wait_send()
    tp_wait(shid.at[:, wide], sh_sems.at[0], sh_sems.at[1]).wait_send()

    @pl.loop(0, sp_count)
    def _(i):
        e = target(i)
        tp_wait(hid.at[e, :, wide], hid_send.at[e], hid_recv.at[e]).wait_send()

        @pl.when(i == 1)
        def _():
            sp_copy(picked_full, picked_full, z_send.at[e], z_recv.at[e], e).wait_send()

        @pl.when(i >= CORES)
        def _():
            sp_copy(picks.at[e], picks.at[e], z_send.at[e], z_recv.at[e], e).wait_send()
            tp_wait(arrived.at[e, :, wide], fwd_send.at[e], fwd_recv.at[e]).wait_send()

        @pl.when(i > 0)
        def _():
            sp_copy(eout.at[e], eout.at[e], ret_send.at[e], ret_recv.at[e], e).wait_send()


def expert_layer(stream, routes, route_weights, norm_gain, gate, up, down, sgate, sup, sdown):
    sp_count = lax.axis_size("sp")
    tp_count = lax.axis_size("tp")
    rows, width = stream.shape
    depth = width * tp_count
    cap = 2 * rows * TOP_K // sp_count
    bf16 = jnp.bfloat16
    vmem = pl.BlockSpec(memory_space=pltpu.VMEM)
    hbm = pl.BlockSpec(memory_space=pl.ANY)
    dma = pltpu.SemaphoreType.DMA
    return pl.pallas_call(
        functools.partial(expert_kernel, sp_count, tp_count, cap),
        out_shape=jax.ShapeDtypeStruct((rows, width), bf16),
        in_specs=[vmem] * 5 + [hbm] * 6,
        out_specs=vmem,
        scratch_shapes=[
            pltpu.VMEM((depth, 2 * width), bf16),
            pltpu.VMEM((depth, width), bf16),
            pltpu.VMEM((depth, 2 * width), bf16),
            pltpu.VMEM((depth, width), bf16),
            pltpu.VMEM((rows, depth), bf16),
            pltpu.VMEM((sp_count, cap, width), bf16),
            pltpu.VMEM((cap, depth), bf16),
            pltpu.VMEM((sp_count, cap, depth), bf16),
            pltpu.VMEM((sp_count, cap, depth), bf16),
            pltpu.VMEM((rows, depth), bf16),
            pltpu.VMEM((sp_count, cap, width), bf16),
            pltpu.VMEM((sp_count, cap, width), bf16),
            pltpu.VMEM((sp_count, rows), jnp.int32),
            pltpu.VMEM((rows, width), jnp.float32),
            dma((6,)),
            dma((2,)),
            dma((sp_count,)),
            dma((sp_count,)),
            dma((sp_count,)),
            dma((sp_count,)),
            dma((sp_count,)),
            dma((sp_count,)),
            dma((2,)),
            dma((sp_count,)),
            dma((sp_count,)),
        ],
        compiler_params=pltpu.CompilerParams(
            collective_id=0, has_side_effects=True, vmem_limit_bytes=56 * 1024 * 1024
        ),
    )(
        stream,
        routes,
        routes.T,
        route_weights,
        norm_gain[:, None],
        gate,
        up,
        down,
        sgate,
        sup,
        sdown,
    )


def per_device(
    queries,
    keys_values,
    sink_logits,
    proj_weight,
    residual,
    norm_gain,
    routes,
    route_weights,
    gate_weight,
    up_weight,
    down_weight,
    shared_gate,
    shared_up,
    shared_down,
):
    tp_index = lax.axis_index("tp")
    sp_index = lax.axis_index("sp")
    sp_count = lax.axis_size("sp")
    tp_count = lax.axis_size("tp")
    heads_here = sink_logits.shape[0]
    col_width = residual.shape[1]
    blocks = TOK_DEV // WINDOW
    kv_group = HEADS // KV_HEADS
    earlier_keys = passed_along(keys_values[:, TOK_DEV - WINDOW :, :], "sp", 1)
    extended = jnp.concatenate([earlier_keys, keys_values], axis=1)
    extended = extended.reshape(2, TOK_DEV + WINDOW, KV_HEADS, HEAD_WIDTH)
    head_ids = tp_index * heads_here + jnp.arange(heads_here, dtype=jnp.int32)
    chosen = jnp.take(extended, head_ids // kv_group, axis=2)
    earlier = chosen[:, :TOK_DEV].reshape(2, blocks, WINDOW, heads_here, HEAD_WIDTH)
    later = chosen[:, WINDOW:].reshape(2, blocks, WINDOW, heads_here, HEAD_WIDTH)
    banded = jnp.concatenate([earlier, later], axis=2)
    query_blocks = queries.reshape(blocks, WINDOW, heads_here, HEAD_WIDTH)
    score_matrix = jnp.einsum(
        "bqhd,bkhd->bhqk", query_blocks, banded[0], preferred_element_type=jnp.float32
    ) * HEAD_WIDTH ** (-0.5)
    query_pos = jnp.arange(WINDOW, dtype=jnp.int32)[:, None]
    key_pos = jnp.arange(2 * WINDOW, dtype=jnp.int32)[None, :]
    distance = WINDOW + query_pos - key_pos
    absolute = (
        sp_index * TOK_DEV
        + jnp.arange(blocks, dtype=jnp.int32)[:, None, None] * WINDOW
        - WINDOW
        + key_pos[None]
    )
    allowed = (distance >= 0)[None] & (distance < WINDOW)[None] & (absolute >= 0)
    masked = jnp.where(allowed[:, None], score_matrix, -jnp.inf)
    sink_value = sink_logits[None, :, None, None]
    highest = jnp.maximum(jnp.max(masked, axis=-1, keepdims=True), sink_value)
    weights_exp = jnp.exp(masked - highest)
    denominator = jnp.sum(weights_exp, axis=-1, keepdims=True) + jnp.exp(sink_value - highest)
    softmax_weights = (weights_exp / denominator).astype(jnp.bfloat16)
    attended_values = jnp.einsum(
        "bhqk,bkhd->bqhd", softmax_weights, banded[1], preferred_element_type=jnp.float32
    )
    attended_values = attended_values.astype(jnp.bfloat16).reshape(TOK_DEV, heads_here * HEAD_WIDTH)
    attended_all = lax.all_gather(attended_values, "tp", axis=1, tiled=True)
    weight_rows = proj_weight.shape[0]
    column_share = lax.all_to_all(
        proj_weight.reshape(weight_rows, tp_count, col_width),
        "tp",
        split_axis=1,
        concat_axis=0,
        tiled=True,
    )
    column_share = column_share.reshape(HEADS * HEAD_WIDTH, col_width)
    feature_sum = jnp.dot(attended_all, column_share, preferred_element_type=jnp.float32)
    stream_cols = (feature_sum + residual.astype(jnp.float32)).astype(jnp.bfloat16)
    return expert_layer(
        stream_cols,
        routes,
        route_weights,
        norm_gain,
        gate_weight,
        up_weight,
        down_weight,
        shared_gate,
        shared_up,
        shared_down,
    )


def solution(mesh):
    placed = (
        P("sp", "tp"),
        P(None, "sp", None),
        P("tp"),
        P("tp", None),
        P("sp", "tp"),
        P(),
        P("sp", None),
        P("sp", None),
        P("sp", None, "tp"),
        P("sp", None, "tp"),
        P("sp", None, "tp"),
        P(None, "tp"),
        P(None, "tp"),
        P(None, "tp"),
    )
    return jax.shard_map(
        per_device, mesh=mesh, in_specs=placed, out_specs=P("sp", "tp"), check_vma=False
    )
```

time: 294 us -> 152 us (0.52)
  Pallas kernels: 0 us -> 115 us
  blocking collectives: 111 us -> 15.8 us
  waiting for transfers between devices: 92.4 us -> 0.01 us
  matrix products: 25.3 us -> 1.86 us
  local copies, waits for them, and re-layouts: 30.1 us -> 9.8 us
  between operations: 13.5 us -> 0.22 us
  other arithmetic: 8.46 us -> 0.78 us
  starting transfers between devices: 12.4 us -> 7.2 us
    pallas_call x0 -> x1, Pallas kernels: none -> 115 us  [expert_layer(): pl.pallas_call(functools.partial(expert_kernel, sp_count, tp_count, cap),...]
    all_to_all x1 -> x0, blocking collectives: 98.4 us -> none  [per_device(): lax.all_to_all(picked_rows.reshape(EXP_DEV, sp_count, capacity, stream_ro...]
    all_gather x3 -> x0, waiting for transfers between devices: 70.6 us -> none  [the longest x1 50.3 us: per_device(): routed_piece = lax.all_gather(hidden, 'tp', axis=2, tiled=True)]
    all_to_all x1 -> x0, waiting for transfers between devices: 21.8 us -> none  [per_device(): lax.all_to_all(outgoing, 'sp', split_axis=1, concat_axis=1, tiled=True)]
    dot_general x7 -> x0, matrix products: 21 us -> none  [the longest x1 5.49 us: per_device(): jnp.einsum('erf,efd->erd', routed_piece, down_weight, preferred_element_t...]
    gather x3 -> x0, local copies, waits for them, and re-layouts: 13.7 us -> none  [the longest x1 10.2 us: per_device(): jnp.take(stream_rows, slot_owner, axis=0, mode='fill', fill_value=0)]
    all_to_all x1 -> x0, starting transfers between devices: 4.61 us -> none  [per_device(): lax.all_to_all(outgoing, 'sp', split_axis=1, concat_axis=1, tiled=True)]
    all_gather x1, blocking collectives: 12.7 us -> 15.8 us  [per_device(): attended_all = lax.all_gather(attended_values, 'tp', axis=1, tiled=True)]
  transfers between devices with their start and end apart: 6 -> 2, of which waited for: 3 -> 0; matrix products, arithmetic and copies ran while one was open for 10% -> 5% of each run, Pallas kernels for 0% -> 0%
where the time goes in v1:
time: 152 us; the launch traced here: 151 us
  Pallas kernels  115 us (76%)
  blocking collectives  15.8 us (10%)
  local copies, waits for them, and re-layouts  9.8 us (6%)
  starting transfers between devices  7.2 us (5%)
  matrix products  1.86 us (1%)
    pallas_call x1, Pallas kernels, expert_layer(): pl.pallas_call(functools.partial(expert_kernel, sp_count, tp_count, cap),...  115 us
    all_gather x1, blocking collectives, per_device(): attended_all = lax.all_gather(attended_values, 'tp', axis=1, tiled=True)  15.8 us
    unnamed x19, local copies, waits for them, and re-layouts  6.71 us
    all_to_all x1, starting transfers between devices, per_device(): lax.all_to_all(proj_weight.reshape(weight_rows, tp_count, col_width), 'tp...  4.67 us
  transfers between devices with their start and end apart: 2, of which 0 were waited for; matrix products, arithmetic and copies ran while one was open for 5% of the time, Pallas kernels for 0%

profile of v1, /device:TPU:0, one launch (start us, length us, event | category | flops | bytes accessed | tf_op | source)
XLA Modules:
  0.0 150.8 jit_solution(7050748823856894203)
XLA Ops:
  0.0 1.1 copy.32
  1.1 0.0 copy-start
  1.1 0.0 copy-start.1
  1.1 2.5 %collective-permute-start = (bf16[2,128,256]{1,2,0:T(8,128)(2,1)S(1)}, bf16[2,128,256]{1,2,0:T(8,128)(2,1)S(1)}, u32[]{:S(2)}, u32[]{:S(2)}) collective-permute-start(bf16[2,128,256]{1,2,0:T(8,128)(2,1)S(1)} %slice.22), channel_id=1, source_target_pairs={{0,4},{4,8},{8,12},{12,16},{16,20},{20,24},{24,28},{1,5},{5,9},{9,... | collective-permute-start | bytes 393224 | tf_op jit(solution)/shard_map/ppermute | solution.py:26
  3.7 2.3 %copy.42 = bf16[256,2048]{0,1:T(8,128)(2,1)} copy(bf16[256,2048]{1,0:T(8,128)(2,1)} %param.17) | data formatting | bytes 2097152 | tf_op args[3]
  6.0 4.7 %all-to-all-start = ((bf16[256,4,512]{0,2,1:T(8,128)(2,1)}), bf16[256,4,512]{0,2,1:T(8,128)(2,1)S(1)}, u32[]{:S(2)}, u32[]{:S(2)}) async-start(bf16[256,4,512]{0,2,1:T(8,128)(2,1)} %bitcast.7), calls=%async_computation | async-start | bytes 2097152 | tf_op jit(solution)/shard_map/all_to_all | solution.py:445
  10.7 0.1 add_compare_fusion
  10.8 0.1 broadcast_and_fusion
  10.9 0.2 reshape.184
  11.1 1.4 copy.46.gain_ref
  12.5 0.8 copy.44.routes_ref
  13.3 0.8 copy.45.weights_ref
  14.1 0.1 pad_maximum_fusion
  14.1 0.6 gather_fusion
  14.8 0.1 select_bitcast_fusion
  14.9 0.1 fusion.10
  15.0 0.0 copy-start.4
  15.0 0.1 reshape.182
  15.1 0.1 reshape.183
  15.2 0.1 copy_dynamic-update-slice_fusion
  15.2 0.4 fusion.11
  15.6 0.1 broadcast_maximum_fusion
  15.7 0.2 fusion.4
  15.9 0.1 exponential_add_fusion
  15.9 0.3 fusion.3
  16.3 0.0 copy-start.5
  16.3 0.1 copy.41
  16.5 15.8 %all_gather.3 = bf16[256,1024]{0,1:T(8,128)(2,1)S(1)} all-gather(bf16[256,256]{0,1:T(8,128)(2,1)S(1)} %bitcast.46), channel_id=1, replica_groups=mesh['sp'=8,'tp'=4] {'tp'}, dimensions={1}, use_global_device_ids=true | all-gather | bytes 655360 | tf_op jit(solution)/shard_map/all_gather | solution.py:443
  32.2 0.5 copy.43
  32.8 1.2 fusion.2.stream_ref
  34.0 115.1 %shard_map.136 = bf16[256,512]{1,0:T(8,128)(2,1)} custom-call(bf16[256,512]{1,0:T(8,128)(2,1)} %fusion.2.stream_ref, s32[256,2]{1,0:T(8,128)} %copy.44.routes_ref, s32[2,256]{1,0:T(2,128)} %bitcast.49, f32[256,2]{1,0:T(8,128)} %copy.45.weights_ref, f32[2048,1]{1,0:T(8,128)} %copy.46.gain_ref, bf16[1,2048,512]{2,1,0:T(8,128)(2,1)} %gate_ref.1, ...), custom_call_target="tpu_custom_call" | custom-call | tf_op jit(solution)/shard_map/pallas_call | solution.py:337
  149.1 1.7 %copy.65 = bf16[256,512]{1,0:T(8,128)(2,1)} copy(bf16[256,512]{1,0:T(8,128)(2,1)} %shard_map.136) | data formatting | bytes 524288
  (19 shorter events, 0.2 us)
Async XLA Ops:
  1.1 9.8 %copy-start = (bf16[256,256]{1,0:T(8,128)(2,1)S(1)}, bf16[256,256]{1,0:T(8,128)(2,1)}, u32[]{:S(2)}) copy-start(bf16[256,256]{1,0:T(8,128)(2,1)} %param.14) | copy-start | bytes 393220
  1.1 10.0 %copy-start.1 = (f32[2048]{0:T(1024)S(1)}, f32[2048]{0:T(1024)}, u32[]{:S(2)}) copy-start(f32[2048]{0:T(1024)} %param.19) | copy-start | bytes 24580
  1.1 12.9 %collective-permute-start = (bf16[2,128,256]{1,2,0:T(8,128)(2,1)S(1)}, bf16[2,128,256]{1,2,0:T(8,128)(2,1)S(1)}, u32[]{:S(2)}, u32[]{:S(2)}) collective-permute-start(bf16[2,128,256]{1,2,0:T(8,128)(2,1)S(1)} %slice.22), channel_id=1, source_target_pairs={{0,4},{4,8},{8,12},{12,16},{16,20},{20,24},{24,28},{1,5},{5,9},{9,... | collective-permute-start | bytes 393224 | tf_op jit(solution)/shard_map/ppermute | solution.py:26
  6.0 6.5 %copy-start.2 = (s32[256,2]{0,1:T(2,128)S(1)}, s32[256,2]{0,1:T(2,128)}, u32[]{:S(2)}) copy-start(s32[256,2]{0,1:T(2,128)} %param.20) | copy-start | bytes 6148
  6.0 7.3 %copy-start.3 = (f32[256,2]{0,1:T(2,128)S(1)}, f32[256,2]{0,1:T(2,128)}, u32[]{:S(2)}) copy-start(f32[256,2]{0,1:T(2,128)} %param.21) | copy-start | bytes 6148
  6.0 26.3 %all-to-all-start = ((bf16[256,4,512]{0,2,1:T(8,128)(2,1)}), bf16[256,4,512]{0,2,1:T(8,128)(2,1)S(1)}, u32[]{:S(2)}, u32[]{:S(2)}) async-start(bf16[256,4,512]{0,2,1:T(8,128)(2,1)} %bitcast.7), calls=%async_computation | async-start | bytes 2097152 | tf_op jit(solution)/shard_map/all_to_all | solution.py:445
  15.0 0.7 copy-start.4
  16.3 16.5 %copy-start.5 = (bf16[256,512]{1,0:T(8,128)(2,1)S(1)}, bf16[256,512]{1,0:T(8,128)(2,1)}, u32[]{:S(2)}) copy-start(bf16[256,512]{1,0:T(8,128)(2,1)} %param.18) | copy-start | bytes 786436

commit v2 on v1

v2 whole, which is shorter than its diff:
```python
import functools

import jax
import jax.numpy as jnp
from jax import lax
from jax.experimental import pallas as pl
from jax.experimental.pallas import tpu as pltpu
from jax.sharding import PartitionSpec as P

D = 2048
HEADS = 16
KV_HEADS = 4
HEAD_WIDTH = 64
WINDOW = 128
TOP_K = 2


norm_eps = 1e-06


MESH = pl.DeviceIdType.MESH
CORES = 2
NEAR = 4
LAG = 3


def expert_kernel(
    sp_count,
    tp_count,
    cap,
    queries_ref,
    kv_ref,
    sink_ref,
    residual_ref,
    routes_row_ref,
    weights_row_ref,
    gain_ref,
    proj_ref,
    gate_ref,
    up_ref,
    down_ref,
    sgate_ref,
    sup_ref,
    sdown_ref,
    out_ref,
    wgu,
    wd,
    sgu,
    sd,
    full,
    picks,
    picked_full,
    arrived,
    hid,
    shid,
    eout,
    returned,
    pos,
    acc,
    stream_ref,
    halo,
    banded,
    attended,
    columns,
    load_sem,
    front_send,
    front_recv,
    stream_send,
    stream_recv,
    z_send,
    z_recv,
    fwd_send,
    fwd_recv,
    hid_send,
    hid_recv,
    sh_send,
    sh_recv,
    ret_send,
    ret_recv,
):
    s = lax.axis_index("sp")
    t = lax.axis_index("tp")
    rows, width = residual_ref.shape
    depth = width * tp_count
    chips = sp_count // CORES
    z, core = s // CORES, lax.rem(s, CORES)
    cols = pl.ds(pl.multiple_of(t * width, width), width)
    wide = pl.ds(0, (tp_count - 1) * width)

    def offset(i):
        step = i // CORES
        return (step + 1) // 2 * (2 * lax.rem(step, 2) - 1)

    def source(i):
        return lax.rem(z + offset(i) + chips, chips) * CORES + lax.rem(
            core + lax.rem(i, CORES), CORES
        )

    def target(i):
        return lax.rem(z - offset(i) + chips, chips) * CORES + lax.rem(
            core - lax.rem(i, CORES) + CORES, CORES
        )

    square = tp_count == 4
    near = min(NEAR, sp_count)
    beside = 2 * (t // 2) + 1 - lax.rem(t, 2)
    across = lax.rem(t + 2, tp_count)

    def shard(n):
        return pl.ds(pl.multiple_of(n * width, width), width)

    def tp_copy(ref, send_sem, recv_sem, device):
        return pltpu.make_async_remote_copy(
            src_ref=ref,
            dst_ref=ref,
            send_sem=send_sem,
            recv_sem=recv_sem,
            device_id={"tp": device},
            device_id_type=MESH,
        )

    def tp_start(ref, send_sem, recv):
        mine = ref.at[:, cols]
        if square:
            tp_copy(mine, send_sem, recv.at[0], beside).start()
            tp_copy(mine, send_sem, recv.at[1], across).start()
        else:
            for j in range(1, tp_count):
                tp_copy(mine, send_sem, recv.at[2], lax.rem(t + j, tp_count)).start()

    def tp_relay(ref, send_sem, recv):
        if square:
            half = ref.shape[0] // 2
            tp_copy(ref.at[:, shard(beside)], send_sem, recv.at[0], beside).wait_recv()
            first = ref.at[pl.ds(0, half), shard(beside)]
            tp_copy(first, send_sem, recv.at[2], across).start()
            tp_copy(ref.at[:, shard(across)], send_sem, recv.at[1], across).wait_recv()
            second = ref.at[pl.ds(half, half), shard(across)]
            tp_copy(second, send_sem, recv.at[2], beside).start()

    def tp_finish(ref, send_sem, recv):
        part = ref.at[:, cols] if square else ref.at[:, wide]
        tp_copy(part, send_sem, recv.at[2], across).wait_recv()

    def tp_sent(ref, send_sem, recv):
        tp_copy(ref.at[:, wide], send_sem, recv.at[2], across).wait_send()

    def sp_copy(src, dst, send_sem, recv_sem, device):
        return pltpu.make_async_remote_copy(
            src_ref=src,
            dst_ref=dst,
            send_sem=send_sem,
            recv_sem=recv_sem,
            device_id={"sp": device},
            device_id_type=MESH,
        )

    lanes = proj_ref.shape[0]
    left, right = pl.ds(0, width), pl.ds(width, width)
    loads = [
        pltpu.make_async_copy(src, dst, load_sem.at[n])
        for n, (src, dst) in enumerate(
            (
                (gate_ref.at[0], wgu.at[:, left]),
                (up_ref.at[0], wgu.at[:, right]),
                (sgate_ref, sgu.at[:, left]),
                (sup_ref, sgu.at[:, right]),
                (down_ref.at[0], wd),
                (sdown_ref, sd),
                (proj_ref.at[:, cols], columns.at[pl.ds(t * lanes, lanes), :]),
            )
        )
    ]
    for load in loads[-1:] + loads[:-1]:
        load.start()

    barrier = pltpu.get_barrier_semaphore()
    for j in range(1, tp_count):
        pl.semaphore_signal(
            barrier, inc=1, device_id={"tp": lax.rem(t + j, tp_count)}, device_id_type=MESH
        )

    @pl.loop(1, sp_count)
    def _(i):
        pl.semaphore_signal(
            barrier, inc=1, device_id={"sp": lax.rem(s + i, sp_count)}, device_id_type=MESH
        )

    named = lax.broadcasted_iota(jnp.int32, (sp_count, rows), 0)
    member = named == routes_row_ref[0:1, :]
    for k in range(1, routes_row_ref.shape[0]):
        member = member | (named == routes_row_ref[k : k + 1, :])
    earlier = lax.broadcasted_iota(jnp.int32, (rows, rows), 0) < lax.broadcasted_iota(
        jnp.int32, (rows, rows), 1
    )
    rank = jnp.dot(
        jnp.where(member, 1.0, 0.0).astype(jnp.bfloat16),
        jnp.where(earlier, 1.0, 0.0).astype(jnp.bfloat16),
        preferred_element_type=jnp.float32,
    )
    pos[...] = jnp.where(member, rank.astype(jnp.int32), -1)

    def chooser(e):
        hit = lax.broadcasted_iota(jnp.int32, (cap, rows), 0) == pos[pl.ds(e, 1), :]
        return jnp.where(hit, 1.0, 0.0).astype(jnp.bfloat16)

    pl.semaphore_wait(barrier, sp_count + tp_count - 2)

    for j in range(1, tp_count):
        peer = lax.rem(t + j, tp_count)
        pltpu.make_async_remote_copy(
            src_ref=proj_ref.at[:, shard(peer)],
            dst_ref=columns.at[pl.ds(t * lanes, lanes), :],
            send_sem=front_send.at[1],
            recv_sem=front_recv.at[1],
            device_id={"tp": peer},
            device_id_type=MESH,
        ).start()

    kv_width = kv_ref.shape[2]
    blocks = rows // WINDOW
    following = lax.rem(s + 1, sp_count)
    tail_copy = sp_copy(
        kv_ref.at[:, pl.ds(rows - WINDOW, WINDOW), :],
        halo,
        front_send.at[0],
        front_recv.at[0],
        following,
    )

    @pl.when(s < sp_count - 1)
    def _():
        tail_copy.start()

    @pl.when(s == 0)
    def _():
        halo[...] = jnp.zeros_like(halo)

    @pl.when(s > 0)
    def _():
        tail_copy.wait_recv()

    heads_here = sink_ref.shape[1]
    kv_group = HEADS // KV_HEADS
    query_pos = lax.broadcasted_iota(jnp.int32, (WINDOW, 2 * WINDOW), 0)
    key_pos = lax.broadcasted_iota(jnp.int32, (WINDOW, 2 * WINDOW), 1)
    distance = WINDOW + query_pos - key_pos
    inside = (distance >= 0) & (distance < WINDOW)
    for head in range(heads_here):
        if head % kv_group == 0:
            kv_head = (t * heads_here + head) // kv_group
            for ref, first, count in ((halo, 0, WINDOW), (kv_ref, WINDOW, rows)):
                chosen = ref[:, :, :HEAD_WIDTH].astype(jnp.float32)
                for n in range(1, kv_width // HEAD_WIDTH):
                    other = ref[:, :, n * HEAD_WIDTH : (n + 1) * HEAD_WIDTH].astype(jnp.float32)
                    chosen = jnp.where(kv_head == n, other, chosen)
                banded[:, first : first + count, :] = chosen.astype(jnp.bfloat16)
        for block in range(blocks):
            here = slice(block * WINDOW, (block + 1) * WINDOW)
            near_keys = slice(block * WINDOW, (block + 2) * WINDOW)
            lane = slice(head * HEAD_WIDTH, (head + 1) * HEAD_WIDTH)
            scores = lax.dot_general(
                queries_ref[here, lane],
                banded[0, near_keys, :],
                (((1,), (1,)), ((), ())),
                preferred_element_type=jnp.float32,
            ) * HEAD_WIDTH ** (-0.5)
            allowed = inside & (key_pos + (s * rows + (block - 1) * WINDOW) >= 0)
            masked = jnp.where(allowed, scores, -jnp.inf)
            sink = sink_ref[0:1, head : head + 1]
            highest = jnp.maximum(jnp.max(masked, axis=-1, keepdims=True), sink)
            raised = jnp.exp(masked - highest)
            total = jnp.sum(raised, axis=-1, keepdims=True) + jnp.exp(sink - highest)
            attended[t, here, lane] = jnp.dot(
                (raised / total).astype(jnp.bfloat16),
                banded[1, near_keys, :],
                preferred_element_type=jnp.float32,
            ).astype(jnp.bfloat16)

    mine = attended.at[t]
    for j in range(1, tp_count):
        tp_copy(mine, front_send.at[2], front_recv.at[2], lax.rem(t + j, tp_count)).start()
    others = attended.at[pl.ds(0, tp_count - 1)]
    attended_wait = tp_copy(others, front_send.at[2], front_recv.at[2], across)
    most = columns.at[pl.ds(0, (tp_count - 1) * lanes), :]
    columns_wait = tp_copy(most, front_send.at[1], front_recv.at[1], across)

    def scale_weights(w):
        step = 128

        @pl.loop(0, depth // step)
        def _(r):
            part = pl.ds(pl.multiple_of(r * step, step), step)
            gain = jnp.broadcast_to(gain_ref[pl.ds(r, 1), :], (step, step)).T
            for n in range(w.shape[1] // step):
                lane = slice(n * step, (n + 1) * step)
                w[part, lane] = (gain * w[part, lane].astype(jnp.float32)).astype(jnp.bfloat16)

    loads[0].wait()
    loads[1].wait()
    scale_weights(wgu)
    loads[6].wait()
    columns_wait.wait_recv()
    attended_wait.wait_recv()
    summed = residual_ref[...].astype(jnp.float32)
    product = jnp.dot(attended[0], columns[:lanes, :], preferred_element_type=jnp.float32)
    for n in range(1, tp_count):
        product += jnp.dot(
            attended[n],
            columns[n * lanes : (n + 1) * lanes, :],
            preferred_element_type=jnp.float32,
        )
    stream_ref[...] = (product + summed).astype(jnp.bfloat16)
    full[:, cols] = stream_ref[...]

    stream = (full, stream_send.at[0], stream_recv.at[0])
    tp_start(*stream)

    @pl.loop(near, sp_count)
    def _(i):
        e = target(i)
        picks[e] = jnp.dot(
            chooser(e), stream_ref[...], preferred_element_type=jnp.float32
        ).astype(jnp.bfloat16)
        sp_copy(picks.at[e], arrived.at[s, :, cols], z_send.at[e], z_recv.at[s], e).start()

    loads[2].wait()
    loads[3].wait()
    scale_weights(sgu)
    tp_relay(*stream)
    tp_finish(*stream)

    @pl.loop(1, near)
    def _(i):
        e = target(i)
        picked_full[i - 1] = jnp.dot(
            chooser(e), full[...], preferred_element_type=jnp.float32
        ).astype(jnp.bfloat16)
        sp_copy(picked_full.at[i - 1], arrived.at[s], z_send.at[e], z_recv.at[s], e).start()

    arrived[s] = jnp.dot(chooser(s), full[...], preferred_element_type=jnp.float32).astype(
        jnp.bfloat16
    )

    def gated(x, w):
        wide_x = x.astype(jnp.float32)
        scale = lax.rsqrt(jnp.sum(wide_x * wide_x, axis=-1, keepdims=True) / depth + norm_eps)
        sums = jnp.dot(x, w[...], preferred_element_type=jnp.float32)
        gate = scale * sums[:, :width]
        return (gate / (1.0 + jnp.exp(-gate)) * (scale * sums[:, width:])).astype(jnp.bfloat16)

    def hidden(src):
        return hid.at[src], hid_send.at[src], hid_recv.at[src]

    def passed(src):
        return arrived.at[src], fwd_send.at[src], fwd_recv.at[src]

    shared = (shid, sh_send.at[0], sh_recv.at[0])

    def hidden_of(src):
        hid[src, :, cols] = gated(arrived[src], wgu)
        tp_start(*hidden(src))

    def pass_on(src):
        mine = arrived.at[src, :, cols]
        sp_copy(mine, mine, z_send.at[src], z_recv.at[src], src).wait_recv()
        tp_start(*passed(src))

    hidden_of(s)
    half = rows // 2

    @pl.loop(0, 2)
    def _(h):
        part = pl.ds(pl.multiple_of(h * half, half), half)
        shid[part, cols] = gated(full[part, :], sgu)

    tp_start(*shared)
    if near < sp_count:
        pass_on(source(near))
    loads[4].wait()
    loads[5].wait()

    @pl.loop(1, sp_count + LAG)
    def _(i):
        @pl.when(i + near < sp_count)
        def _():
            pass_on(source(i + near))

        @pl.when((i + near - 1 >= near) & (i + near - 1 < sp_count))
        def _():
            tp_relay(*passed(source(i + near - 1)))

        @pl.when(i < sp_count)
        def _():
            src = source(i)

            @pl.when(i < near)
            def _():
                mine = arrived.at[src]
                sp_copy(mine, mine, z_send.at[src], z_recv.at[src], src).wait_recv()

            @pl.when(i >= near)
            def _():
                tp_finish(*passed(src))

            hidden_of(src)

        @pl.when(i <= sp_count)
        def _():
            tp_relay(*hidden(source(i - 1)))

        @pl.when(i == 1)
        def _():
            tp_relay(*shared)

        @pl.when(i >= LAG)
        def _():
            src = source(i - LAG)
            tp_finish(*hidden(src))
            result = jnp.dot(hid[src], wd[...], preferred_element_type=jnp.float32).astype(
                jnp.bfloat16
            )

            @pl.when(i == LAG)
            def _():
                returned[s] = result

            @pl.when(i > LAG)
            def _():
                eout[src] = result
                sp_copy(
                    eout.at[src], returned.at[s], ret_send.at[src], ret_recv.at[s], src
                ).start()

    tp_finish(*shared)
    acc[...] = stream_ref[...].astype(jnp.float32) + jnp.dot(
        shid[...], sd[...], preferred_element_type=jnp.float32
    )

    @pl.loop(0, sp_count)
    def _(i):
        e = target(i)

        @pl.when(i > 0)
        def _():
            mine = returned.at[e]
            sp_copy(mine, mine, ret_send.at[e], ret_recv.at[e], e).wait_recv()

        picked = lax.dot_general(
            chooser(e), returned[e], (((0,), (0,)), ((), ())), preferred_element_type=jnp.float32
        )
        weight = jnp.sum(
            jnp.where(routes_row_ref[...] == e, weights_row_ref[...], 0.0), axis=0, keepdims=True
        )
        spread = jnp.broadcast_to(weight, (128, rows)).T
        for n in range(width // 128):
            lane = slice(n * 128, (n + 1) * 128)
            acc[:, lane] += spread * picked[:, lane]

    out_ref[...] = acc[...].astype(out_ref.dtype)

    tp_sent(*stream)
    columns_wait.wait_send()
    attended_wait.wait_send()

    @pl.when(s < sp_count - 1)
    def _():
        tail_copy.wait_send()

    tp_sent(*shared)

    @pl.loop(0, sp_count)
    def _(i):
        e = target(i)
        tp_sent(*hidden(e))

        @pl.when((i > 0) & (i < near))
        def _():
            mine = picked_full.at[i - 1]
            sp_copy(mine, mine, z_send.at[e], z_recv.at[e], e).wait_send()

        @pl.when(i >= near)
        def _():
            sp_copy(picks.at[e], picks.at[e], z_send.at[e], z_recv.at[e], e).wait_send()

            tp_sent(*passed(source(i)))

        @pl.when(i > 0)
        def _():
            sp_copy(eout.at[e], eout.at[e], ret_send.at[e], ret_recv.at[e], e).wait_send()


def per_device(
    queries,
    keys_values,
    sink_logits,
    proj_weight,
    residual,
    norm_gain,
    routes,
    route_weights,
    gate_weight,
    up_weight,
    down_weight,
    shared_gate,
    shared_up,
    shared_down,
):
    sp_count = lax.axis_size("sp")
    tp_count = lax.axis_size("tp")
    rows, width = residual.shape
    depth = width * tp_count
    cap = 2 * rows * TOP_K // sp_count
    kv_width = keys_values.shape[2]
    bf16 = jnp.bfloat16
    vmem = pl.BlockSpec(memory_space=pltpu.VMEM)
    hbm = pl.BlockSpec(memory_space=pl.ANY)
    dma = pltpu.SemaphoreType.DMA
    return pl.pallas_call(
        functools.partial(expert_kernel, sp_count, tp_count, cap),
        out_shape=jax.ShapeDtypeStruct((rows, width), bf16),
        in_specs=[vmem] * 7 + [hbm] * 7,
        out_specs=vmem,
        scratch_shapes=[
            pltpu.VMEM((depth, 2 * width), bf16),
            pltpu.VMEM((depth, width), bf16),
            pltpu.VMEM((depth, 2 * width), bf16),
            pltpu.VMEM((depth, width), bf16),
            pltpu.VMEM((rows, depth), bf16),
            pltpu.VMEM((sp_count, cap, width), bf16),
            pltpu.VMEM((max(1, min(NEAR, sp_count) - 1), cap, depth), bf16),
            pltpu.VMEM((sp_count, cap, depth), bf16),
            pltpu.VMEM((sp_count, cap, depth), bf16),
            pltpu.VMEM((rows, depth), bf16),
            pltpu.VMEM((sp_count, cap, width), bf16),
            pltpu.VMEM((sp_count, cap, width), bf16),
            pltpu.VMEM((sp_count, rows), jnp.int32),
            pltpu.VMEM((rows, width), jnp.float32),
            pltpu.VMEM((rows, width), bf16),
            pltpu.VMEM((2, WINDOW, kv_width), bf16),
            pltpu.VMEM((2, WINDOW + rows, HEAD_WIDTH), bf16),
            pltpu.VMEM((tp_count,) + queries.shape, bf16),
            pltpu.VMEM((tp_count * proj_weight.shape[0], width), bf16),
            dma((7,)),
            dma((3,)),
            dma((3,)),
            dma((1,)),
            dma((1, 3)),
            dma((sp_count,)),
            dma((sp_count,)),
            dma((sp_count,)),
            dma((sp_count, 3)),
            dma((sp_count,)),
            dma((sp_count, 3)),
            dma((1,)),
            dma((1, 3)),
            dma((sp_count,)),
            dma((sp_count,)),
        ],
        compiler_params=pltpu.CompilerParams(
            collective_id=0, has_side_effects=True, vmem_limit_bytes=56 * 1024 * 1024
        ),
    )(
        queries,
        keys_values,
        sink_logits[None, :],
        residual,
        routes.T,
        route_weights.T,
        norm_gain.reshape(-1, 128),
        proj_weight,
        gate_weight,
        up_weight,
        down_weight,
        shared_gate,
        shared_up,
        shared_down,
    )


def solution(mesh):
    placed = (
        P("sp", "tp"),
        P(None, "sp", None),
        P("tp"),
        P("tp", None),
        P("sp", "tp"),
        P(),
        P("sp", None),
        P("sp", None),
        P("sp", None, "tp"),
        P("sp", None, "tp"),
        P("sp", None, "tp"),
        P(None, "tp"),
        P(None, "tp"),
        P(None, "tp"),
    )
    return jax.shard_map(
        per_device, mesh=mesh, in_specs=placed, out_specs=P("sp", "tp"), check_vma=False
    )
```

time: 152 us -> 115 us (0.76)
  blocking collectives: 15.8 us -> 0 us
  local copies, waits for them, and re-layouts: 9.8 us -> 1.67 us
  starting transfers between devices: 7.2 us -> 0 us
  Pallas kernels: 115 us -> 113 us
  matrix products: 1.86 us -> 0 us
    all_gather x1 -> x0, blocking collectives: 15.8 us -> none  [per_device(): attended_all = lax.all_gather(attended_values, 'tp', axis=1, tiled=True)]
    unnamed x19 -> x1, local copies, waits for them, and re-layouts: 6.71 us -> 1.67 us
    all_to_all x1 -> x0, starting transfers between devices: 4.67 us -> none  [per_device(): lax.all_to_all(proj_weight.reshape(weight_rows, tp_count, col_width), 'tp...]
    ppermute x1 -> x0, starting transfers between devices: 2.54 us -> none  [passed_along(): lax.ppermute(value, axis, [(source, source + steps) for source in range(i...]
    pallas_call x1, Pallas kernels: 115 us -> 113 us  [per_device(): pl.pallas_call(functools.partial(expert_kernel, sp_count, tp_count, cap),...]
    dot_general x3 -> x0, matrix products: 1.86 us -> none  [the longest x1 1.16 us: per_device(): jnp.dot(attended_all, column_share, preferred_element_type=jnp.float32)]
  transfers between devices with their start and end apart: 2 -> 0, of which waited for: 0 -> 0; matrix products, arithmetic and copies ran while one was open for 5% -> 0% of each run, Pallas kernels for 0% -> 0%
where the time goes in v2:
time: 115 us; the launch traced here: 114 us
  Pallas kernels  113 us (98%)
  local copies, waits for them, and re-layouts  1.67 us (1%)
    pallas_call x1, Pallas kernels, per_device(): pl.pallas_call(functools.partial(expert_kernel, sp_count, tp_count, cap),...  113 us

profile of v2, /device:TPU:0, one launch (start us, length us, event | category | flops | bytes accessed | tf_op | source)
XLA Modules:
  0.0 114.4 jit_solution(15486864543679311312)
XLA Ops:
  0.0 112.7 %shard_map.136 = bf16[256,512]{1,0:T(8,128)(2,1)} custom-call(bf16[256,256]{1,0:T(8,128)(2,1)} %queries_ref.1, bf16[2,256,256]{2,1,0:T(8,128)(2,1)} %kv_ref.1, f32[1,4]{1,0:T(1,128)} %bitcast.7, bf16[256,512]{1,0:T(8,128)(2,1)} %residual_ref.1, s32[2,256]{1,0:T(2,128)} %bitcast.5, f32[2,256]{1,0:T(2,128)} %bitcast.6, f32[16,128]{1,0:T(8,128)} %bitcast.4, ...), custom_call_target="tpu_custom_call" | custom-call | tf_op jit(solution)/shard_map/pallas_call | solution.py:519
  112.7 1.7 %copy.16 = bf16[256,512]{1,0:T(8,128)(2,1)} copy(bf16[256,512]{1,0:T(8,128)(2,1)} %shard_map.136) | data formatting | bytes 524288
